TPU v7x, 512 devices: a whole 4x4x16 slice. The times are simulated.
512 devices in a mesh: ep: 32 (over z, core), tp: 16 (over y, x).
Axes of the slice: x: 4, y: 4, z: 16, core: 2. Of those that a mesh axis runs over, the one named last changes fastest.
Arguments:
- mixer_input: bfloat16 [8192, 2048], P('ep'), may hold values from -6 to 6
- mixer_gain: float32 [2048], replicated, may hold values from 0.1 to 1.9
- query_weight: bfloat16 [2048, 2048], P(None, 'tp'), may hold values from -0.13258252 to 0.13258252
- key_weight: bfloat16 [2048, 1024], P(None, 'tp'), may hold values from -2.78423295 to 2.78423295
- value_weight: bfloat16 [2048, 1024], P(None, 'tp'), may hold values from -0.125 to 0.125
- output_weight: bfloat16 [2048, 2048], P(None, 'tp'), may hold values from -1 to 1
- sink_logit: float32 [32], P('tp'), may hold values from 2 to 7
- expert_input: bfloat16 [4096, 2048], P('ep'), may hold values from -6 to 6
- expert_gain: float32 [2048], replicated, may hold values from 0.1 to 1.9
- routes: int32 [4096, 4], P('ep'), may hold values from 0 to 31, all different within a row; in each aligned block of 128 rows (0 to 127, 128 to 255, ...) at most 32 rows name the same one
- route_logits: float32 [4096, 4], P('ep'), may hold values from -6 to 6
- gate_weight: bfloat16 [32, 2048, 2048], P('ep', None, 'tp'), may hold values from -0.375 to 0.375
- up_weight: bfloat16 [32, 2048, 2048], P('ep', None, 'tp'), may hold values from -0.375 to 0.375
- down_weight: bfloat16 [32, 2048, 2048], P('ep', None, 'tp'), may hold values from -0.03125 to 0.03125
Outputs:
- mixer_output: bfloat16 [8192, 2048], P('ep', 'tp')
- expert_output: bfloat16 [4096, 2048], P('ep', 'tp')
Inputs may be any that keep to these rules, and one draw needn't show every extreme that they name: `routes`: each token names 4 different experts. Among the 128 tokens of one index of ep (aligned blocks) no expert is named more than 32 times, and in some blocks one expert is named exactly 32 times.
All inputs are finite; a program needn't handle non-finite values.
Results may differ from a plain program's by a relative error of at most 0.0055.
The roundings to bfloat16 on the way count: a program that leaves them out, or rounds other values in their place, can miss the bound.
Values may be sent and summed in bfloat16 or wider, within the bound.
No kernel may reach another device: no remote copies, remote signals or barrier semaphores. Data moves between devices by JAX's collectives and lax.ppermute only.
A program may use at most 64 MiB of HBM per device.

v0:
```python
import jax
import jax.numpy as jnp
from jax import lax
from jax.sharding import Mesh
from jax.sharding import PartitionSpec as P

HEAD_DIM = 64
TOP_K = 4
WINDOW = 128
GRID_W = 64
EP = ("ep_0", "ep_1")
EPSILON = 1e-06
LIMIT = 7.0
SLOPE = 1.702
BASE = 10000.0


def extended(shard, sides, width):
    for axis, dim in sides:
        devices, length = (lax.axis_size(axis), shard.shape[dim])
        up = [(i, (i + 1) % devices) for i in range(devices - 1)]
        down = [(j, i) for i, j in up]
        last = lax.slice_in_dim(shard, length - width, length, axis=dim)
        first = lax.slice_in_dim(shard, 0, width, axis=dim)
        before = lax.ppermute(last, axis, up)
        after = lax.ppermute(first, axis, down)
        shard = jnp.concatenate([before, shard, after], axis=dim)
    return shard


def cut_along(shard, dim, devices):
    shape = shard.shape
    pieces = shard.reshape(*shape[:dim], devices, shape[dim] // devices, *shape[dim + 1 :])
    return jnp.moveaxis(pieces, dim, 0)


def joined_along(pieces, dim):
    pieces = jnp.moveaxis(pieces, 0, dim)
    shape = pieces.shape
    return pieces.reshape(*shape[:dim], shape[dim] * shape[dim + 1], *shape[dim + 2 :])


def exchange_in_order(pieces, axes, order):
    inside = pieces.shape[1:]
    whole = pieces.reshape(*(lax.axis_size(a) for a in axes), *inside)
    for k in order:
        whole = lax.all_to_all(whole, axes[k], k, k, tiled=True)
    return whole.reshape(-1, *inside)


def exchange_by_chip(shard, groups, order, split_dim, concat_dim):
    devices = lax.axis_size(groups[0]) * lax.axis_size(groups[1])
    pieces = cut_along(shard, split_dim, devices)
    return joined_along(exchange_in_order(pieces, groups, order), concat_dim)


def side_by_side(arrays, axis, dim, along):
    widths = [a.shape[along] for a in arrays]
    both = jnp.concatenate(arrays, axis=along)
    whole = lax.all_gather(both, axis, axis=dim, tiled=True)
    return tuple(jnp.split(whole, [sum(widths[:k]) for k in range(1, len(widths))], axis=along))


def normalize(rows, gain):
    values = rows.astype(jnp.float32)
    scaled = values * lax.rsqrt(jnp.mean(values * values, axis=-1, keepdims=True) + EPSILON)
    return (scaled * gain).astype(jnp.bfloat16)


def turn(values, cosine, sine):
    first, second = jnp.split(values, 2, axis=-1)
    cosine = cosine[:, None, :]
    sine = sine[:, None, :]
    return jnp.concatenate(
        [first * cosine - second * sine, second * cosine + first * sine], axis=-1
    )


def axial_rope(values, places):
    quarter = values.shape[-1] // 4
    frequency = BASE ** (-jnp.arange(quarter, dtype=jnp.float32) / quarter)
    row_angle = (places // GRID_W).astype(jnp.float32)[:, None] * frequency[None, :]
    column_angle = (places % GRID_W).astype(jnp.float32)[:, None] * frequency[None, :]
    row_part, column_part = jnp.split(values, 2, axis=-1)
    return jnp.concatenate(
        [
            turn(row_part, jnp.cos(row_angle), jnp.sin(row_angle)),
            turn(column_part, jnp.cos(column_angle), jnp.sin(column_angle)),
        ],
        axis=-1,
    )


def activate(gate, up):
    capped = jnp.minimum(gate, LIMIT)
    bounded = jnp.clip(up, -LIMIT, LIMIT)
    return (capped * jax.nn.sigmoid(SLOPE * capped) * (bounded + 1.0)).astype(jnp.bfloat16)


def add_product(piece, weight):
    return jnp.dot(piece, weight, preferred_element_type=jnp.float32)


def shards(
    mixer_input,
    mixer_gain,
    query_weight,
    key_weight,
    value_weight,
    output_weight,
    sink_logit,
    expert_input,
    expert_gain,
    routes,
    route_logits,
    gate_weight,
    up_weight,
    down_weight,
):
    tokens = mixer_input.shape[0]
    query_heads = query_weight.shape[1] // HEAD_DIM
    key_heads = key_weight.shape[1] // HEAD_DIM
    group = query_heads // key_heads
    blocks = tokens // WINDOW
    offset = lax.axis_index(EP) * tokens
    length = lax.axis_size(EP) * tokens
    places = offset + jnp.arange(tokens, dtype=jnp.int32)
    normed = normalize(mixer_input, mixer_gain)
    query = jnp.dot(normed, query_weight, preferred_element_type=jnp.float32).reshape(
        tokens, query_heads, HEAD_DIM
    )
    query = (
        axial_rope(query, places)
        .astype(jnp.bfloat16)
        .reshape(blocks, WINDOW, key_heads, group, HEAD_DIM)
    )
    keys = jnp.dot(normed, key_weight, preferred_element_type=jnp.float32).reshape(
        tokens, key_heads, HEAD_DIM
    )
    keys = axial_rope(keys, places).astype(jnp.bfloat16).reshape(tokens, key_heads * HEAD_DIM)
    values = jnp.dot(normed, value_weight, preferred_element_type=jnp.float32).astype(jnp.bfloat16)
    stacked = jnp.concatenate([keys, values], axis=1)
    widened = extended(stacked, ((EP, 0),), WINDOW)
    framed = widened.reshape(blocks + 2, WINDOW, 2, key_heads, HEAD_DIM)
    nearby = jnp.concatenate([framed[:-2], framed[1:-1], framed[2:]], axis=1)
    scores = jnp.einsum(
        "nqgrd,nkgd->ngrqk", query, nearby[:, :, 0], preferred_element_type=jnp.float32
    ) * HEAD_DIM ** (-0.5)
    query_place = places.reshape(blocks, WINDOW)
    key_place = (
        offset
        + (jnp.arange(blocks, dtype=jnp.int32)[:, None] - 1) * WINDOW
        + jnp.arange(3 * WINDOW, dtype=jnp.int32)[None, :]
    )
    allowed = (
        (jnp.abs(query_place[:, :, None] - key_place[:, None, :]) <= WINDOW)
        & (key_place[:, None, :] >= 0)
        & (key_place[:, None, :] < length)
    )
    scores = jnp.where(allowed[:, None, None], scores, -1e30)
    sinks = sink_logit.reshape(key_heads, group)[None, :, :, None]
    top = jnp.maximum(jnp.max(scores, axis=-1), sinks)
    weights = jnp.exp(scores - top[..., None])
    denominator = jnp.sum(weights, axis=-1) + jnp.exp(sinks - top)
    shares = (weights / denominator[..., None]).astype(jnp.bfloat16)
    mixed = jnp.einsum(
        "ngrqk,nkgd->nqgrd", shares, nearby[:, :, 1], preferred_element_type=jnp.float32
    )
    mixed = mixed.astype(jnp.bfloat16).reshape(tokens, query_heads * HEAD_DIM)
    experts = lax.axis_size(EP)
    rows_here = expert_input.shape[0]
    capacity = 2 * rows_here * TOP_K // experts
    expert_normed = normalize(expert_input, expert_gain)
    chances = jax.nn.softmax(route_logits, axis=-1)
    chosen = routes.reshape(-1)
    marks = (chosen[:, None] == jnp.arange(experts, dtype=jnp.int32)[None, :]).astype(jnp.int32)
    earlier = jnp.sum((jnp.cumsum(marks, axis=0) - marks) * marks, axis=1)
    target = chosen * capacity + earlier
    source = (
        jnp.full((experts * capacity,), rows_here, jnp.int32)
        .at[target]
        .set(jnp.arange(chosen.shape[0], dtype=jnp.int32) // TOP_K)
    )
    padded = jnp.concatenate(
        [expert_normed, jnp.zeros((1, expert_normed.shape[1]), jnp.bfloat16)], axis=0
    )
    down_local = down_weight[0]
    gate_local = gate_weight[0]
    up_local = up_weight[0]
    width = padded.shape[1] // lax.axis_size("tp")
    own = lax.dynamic_slice_in_dim(padded, lax.axis_index("tp") * width, width, 1)
    outgoing = own[source].reshape(experts, capacity, width)
    received = lax.all_to_all(outgoing, EP, split_axis=0, concat_axis=0, tiled=True)
    flat = received.reshape(experts * capacity, width)
    head_piece, feature_piece = side_by_side((mixed, flat), "tp", 1, 0)
    mixer_total = add_product(head_piece, output_weight)
    gate = add_product(feature_piece, gate_local)
    up = add_product(feature_piece, up_local)
    hidden = activate(gate, up)
    result = add_product(lax.all_gather(hidden, "tp", axis=1, tiled=True), down_local)
    result = result.astype(jnp.bfloat16).reshape(experts, capacity, down_local.shape[1])
    returned = exchange_by_chip(result, ("ep_0", "ep_1"), (1, 0), 0, 0)
    mixer_output = mixer_total.astype(jnp.bfloat16)
    results = returned.reshape(experts * capacity, returned.shape[2])
    picked = results[target].astype(jnp.float32).reshape(rows_here, TOP_K, returned.shape[2])
    expert_output = jnp.sum(picked * chances[:, :, None], axis=1).astype(jnp.bfloat16)
    return (mixer_output, expert_output)


def solution(mesh):
    finer = Mesh(mesh.devices.reshape(16, 2, mesh.shape["tp"]), ("ep_0", "ep_1", "tp"))
    in_specs = (
        P(EP, None),
        P(),
        P(None, "tp"),
        P(None, "tp"),
        P(None, "tp"),
        P(None, "tp"),
        P("tp"),
        P(EP, None),
        P(),
        P(EP, None),
        P(EP, None),
        P(EP, None, "tp"),
        P(EP, None, "tp"),
        P(EP, None, "tp"),
    )
    out_specs = (P(EP, "tp"), P(EP, "tp"))
    return jax.shard_map(
        shards, mesh=finer, in_specs=in_specs, out_specs=out_specs, check_vma=False
    )
```

profile of v0, /device:TPU:32, one launch (start us, length us, event | category | flops | bytes accessed | tf_op | source)
XLA Modules:
  0.0 255.0 jit_solution(9797498149042853800)
XLA Ops:
  7.2 0.7 broadcast_multiply_fusion
  7.9 0.8 copy.46
  8.9 1.2 fusion.26
  10.4 1.2 reduce-window.6
  12.0 2.4 scatter_custom_fusion
  14.5 1.3 fusion.28
  15.8 4.3 %gather_fusion = bf16[1024,128]{1,0:T(8,128)(2,1)} fusion(bf16[129,128]{1,0:T(8,128)(2,1)S(1)} %pad_dynamic-slice_fusion, s32[1024]{0:T(1024)S(1)} %fusion.69), kind=kCustom, calls=%fused_computation | custom fusion | bytes 528384 | tf_op jit(solution)/shard_map/gather | solution.py:192
  20.1 15.5 %all-to-all-start = ((bf16[32,32,128]{2,1,0:T(8,128)(2,1)}), bf16[32,32,128]{2,1,0:T(8,128)(2,1)S(1)}, u32[]{:S(2)}, u32[]{:S(2)}) async-start(bf16[32,32,128]{2,1,0:T(8,128)(2,1)} %bitcast.20), calls=%async_computation | async-start | bytes 524288 | tf_op jit(solution)/shard_map/all_to_all | solution.py:193
  37.7 2.0 collective-permute-start.1
  39.7 2.3 collective-permute-start
  43.6 3.0 %collective-permute-done.1 = bf16[128,128]{0,1:T(8,128)(2,1)S(1)} collective-permute-done((bf16[128,128]{0,1:T(8,128)(2,1)S(1)}, bf16[128,128]{0,1:T(8,128)(2,1)S(1)}, u32[]{:S(2)}, u32[]{:S(2)}) %collective-permute-start.1) | collective-permute-done | bytes 32800 | tf_op jit(solution)/shard_map/ppermute | solution.py:26
  47.8 8.7 %all-to-all-done = bf16[32,32,128]{2,1,0:T(8,128)(2,1)S(1)} async-done(((bf16[32,32,128]{2,1,0:T(8,128)(2,1)}), bf16[32,32,128]{2,1,0:T(8,128)(2,1)S(1)}, u32[]{:S(2)}, u32[]{:S(2)}) %all-to-all-start) | async-done | bytes 262176 | tf_op jit(solution)/shard_map/all_to_all | solution.py:193
  56.6 0.7 pad_maximum_fusion
  57.4 71.7 %all-gather.3.cloned.1.call-done = bf16[1280,2048]{1,0:T(8,128)(2,1)} async-done(((bf16[1280,128]{1,0:T(8,128)(2,1)}), bf16[1280,2048]{1,0:T(8,128)(2,1)}) %all-gather.3.cloned.1.call-update) | async-done | bytes 5242896 | tf_op jit(solution)/shard_map/all_gather | solution.py:60
  129.1 3.6 %fusion.8 = f32[1024,128]{1,0:T(8,128)S(1)} fusion(bf16[1280,2048]{1,0:T(8,128)(2,1)} %all-gather.3.cloned.1.call-done, bf16[1,2048,128]{2,1,0:T(8,128)(2,1)S(1)} %copy-done), kind=kOutput, calls=%fused_computation.16 | convolution fusion | flops 537001984 | bytes 5242880 | tf_op jit(solution)/shard_map/dot_general | solution.py:101
  132.8 2.0 fusion.21
  134.8 71.7 %all-gather.5.cloned.1.call-done = bf16[1024,2048]{1,0:T(8,128)(2,1)} async-done(((bf16[1024,128]{1,0:T(8,128)(2,1)}), bf16[1024,2048]{1,0:T(8,128)(2,1)}) %all-gather.5.cloned.1.call-update) | async-done | bytes 4194320 | tf_op jit(solution)/shard_map/all_gather | solution.py:200
  206.6 3.4 %convolution_convert_fusion = bf16[1024,128]{1,0:T(8,128)(2,1)S(1)} fusion(bf16[1024,2048]{1,0:T(8,128)(2,1)} %all-gather.5.cloned.1.call-done, bf16[1,2048,128]{2,1,0:T(8,128)(2,1)S(1)} %copy-done.7), kind=kOutput, calls=%fused_computation.22 | convolution fusion | flops 537001984 | bytes 4980736 | tf_op jit(solution)/shard_map/dot_general | solution.py:101
  210.1 4.1 %all_to_all.15 = bf16[16,2,1,32,128]{4,3,0,2,1:T(8,128)(2,1)S(1)} all-to-all(bf16[16,2,1,32,128]{4,3,0,2,1:T(8,128)(2,1)S(1)} %copy.50), channel_id=1, replica_groups=mesh['ep_0'=16,'ep_1'=2,'tp'=16] {'ep_1'}, dimensions={1} | all-to-all | bytes 524288 | tf_op jit(solution)/shard_map/all_to_all | solution.py:47
  214.9 12.7 %all-to-all-start.2 = ((bf16[16,2,1,32,128]{4,3,1,2,0:T(8,128)(2,1)}), bf16[16,2,1,32,128]{4,3,1,2,0:T(8,128)(2,1)S(1)}, u32[]{:S(2)}, u32[]{:S(2)}) async-start(bf16[16,2,1,32,128]{4,3,1,2,0:T(8,128)(2,1)} %copy.51), calls=%async_computation.2 | async-start | bytes 524288 | tf_op jit(solution)/shard_map/all_to_all | solution.py:47
  227.7 2.3 convolution_convert_fusion.1
  230.0 15.9 %all-to-all-done.2 = bf16[16,2,1,32,128]{4,3,1,2,0:T(8,128)(2,1)S(1)} async-done(((bf16[16,2,1,32,128]{4,3,1,2,0:T(8,128)(2,1)}), bf16[16,2,1,32,128]{4,3,1,2,0:T(8,128)(2,1)S(1)}, u32[]{:S(2)}, u32[]{:S(2)}) %all-to-all-start.2) | async-done | bytes 262176 | tf_op jit(solution)/shard_map/all_to_all | solution.py:47
  245.9 1.3 gather_fusion.1
  247.2 0.9 fusion.37
  (87 shorter events, 6.7 us)
Async XLA Ops:
  7.2 121.9 %copy-start = (bf16[1,2048,128]{2,1,0:T(8,128)(2,1)S(1)}, bf16[1,2048,128]{2,1,0:T(8,128)(2,1)}, u32[]{:S(2)}) copy-start(bf16[1,2048,128]{2,1,0:T(8,128)(2,1)} %param.25) | copy-start | bytes 1572868
  14.4 21.2 %copy-start.1 = (bf16[256,2048]{1,0:T(8,128)(2,1)S(1)}, bf16[256,2048]{1,0:T(8,128)(2,1)}, u32[]{:S(2)}) copy-start(bf16[256,2048]{1,0:T(8,128)(2,1)} %param.14) | copy-start | bytes 3145732
  15.8 20.2 %copy-start.9 = (bf16[2048,64]{0,1:T(8,128)(2,1)S(1)}, bf16[2048,64]{0,1:T(8,128)(2,1)}, u32[]{:S(2)}) copy-start(bf16[2048,64]{0,1:T(8,128)(2,1)} %param.17) | copy-start | bytes 786436
  15.8 20.2 %copy-start.11 = (f32[2048]{0:T(1024)S(1)}, f32[2048]{0:T(1024)}, u32[]{:S(2)}) copy-start(f32[2048]{0:T(1024)} %param.15) | copy-start | bytes 24580
  20.1 17.0 %copy-start.10 = (bf16[2048,64]{0,1:T(8,128)(2,1)S(1)}, bf16[2048,64]{0,1:T(8,128)(2,1)}, u32[]{:S(2)}) copy-start(bf16[2048,64]{0,1:T(8,128)(2,1)} %param.18) | copy-start | bytes 786436
  20.1 36.5 %all-to-all-start = ((bf16[32,32,128]{2,1,0:T(8,128)(2,1)}), bf16[32,32,128]{2,1,0:T(8,128)(2,1)S(1)}, u32[]{:S(2)}, u32[]{:S(2)}) async-start(bf16[32,32,128]{2,1,0:T(8,128)(2,1)} %bitcast.20), calls=%async_computation | async-start | bytes 524288 | tf_op jit(solution)/shard_map/all_to_all | solution.py:193
  35.6 93.5 %all-gather.3.cloned.1.call-start = ((), (), s32[]{:S(2)}) async-start(), calls=%async_computation.3 | async-start | bytes 5570560 | tf_op jit(solution)/shard_map/all_gather | solution.py:60
  36.0 6.4 %copy-start.5 = (bf16[2048,128]{1,0:T(8,128)(2,1)S(1)}, bf16[2048,128]{1,0:T(8,128)(2,1)}, u32[]{:S(2)}) copy-start(bf16[2048,128]{1,0:T(8,128)(2,1)} %param.16) | copy-start | bytes 1572868
  37.7 8.9 %collective-permute-start.1 = (bf16[128,128]{0,1:T(8,128)(2,1)S(1)}, bf16[128,128]{0,1:T(8,128)(2,1)S(1)}, u32[]{:S(2)}, u32[]{:S(2)}) collective-permute-start(bf16[128,128]{0,1:T(8,128)(2,1)S(1)} %get-tuple-element.10), channel_id=1, source_target_pairs={{16,0},{32,16},{48,32},{64,48},{80,64},{96,80},{112,96},{128,112},... | collective-permute-start | bytes 98312 | tf_op jit(solution)/shard_map/ppermute | solution.py:26
  39.7 6.9 %collective-permute-start = (bf16[128,128]{0,1:T(8,128)(2,1)S(1)}, bf16[128,128]{0,1:T(8,128)(2,1)S(1)}, u32[]{:S(2)}, u32[]{:S(2)}) collective-permute-start(bf16[128,128]{0,1:T(8,128)(2,1)S(1)} %get-tuple-element.11), channel_id=1, source_target_pairs={{0,16},{16,32},{32,48},{48,64},{64,80},{80,96},{96,112},{112,128},... | collective-permute-start | bytes 98312 | tf_op jit(solution)/shard_map/ppermute | solution.py:25
  42.4 4.7 %copy-start.3 = (f32[2]{0:T(128)S(1)}, f32[2]{0:T(128)}, u32[]{:S(2)}) copy-start(f32[2]{0:T(128)} %param.20) | copy-start | bytes 28
  57.3 75.3 %copy-start.6 = (bf16[1,2048,128]{2,1,0:T(8,128)(2,1)S(1)}, bf16[1,2048,128]{2,1,0:T(8,128)(2,1)}, u32[]{:S(2)}) copy-start(bf16[1,2048,128]{2,1,0:T(8,128)(2,1)} %param.26) | copy-start | bytes 1572868
  57.4 149.2 %all-gather.5.cloned.1.call-start = ((), (), s32[]{:S(2)}) async-start(), calls=%async_computation.4 | async-start | bytes 4456448 | tf_op jit(solution)/shard_map/all_gather | solution.py:200
  129.1 3.7 %copy-start.4 = (bf16[1280,2048]{1,0:T(8,128)(2,1)S(1)}, bf16[1280,2048]{1,0:T(8,128)(2,1)}, u32[]{:S(2)}) copy-start(bf16[1280,2048]{1,0:T(8,128)(2,1)} %all-gather.3.cloned.1.call-done) | copy-start | bytes 15728644
  132.8 73.7 %copy-start.7 = (bf16[1,2048,128]{2,1,0:T(8,128)(2,1)S(1)}, bf16[1,2048,128]{2,1,0:T(8,128)(2,1)}, u32[]{:S(2)}) copy-start(bf16[1,2048,128]{2,1,0:T(8,128)(2,1)} %param.27) | copy-start | bytes 1572868
  210.0 17.5 %copy-start.2 = (f32[128,4]{0,1:T(4,128)S(1)}, f32[128,4]{0,1:T(4,128)}, u32[]{:S(2)}) copy-start(f32[128,4]{0,1:T(4,128)} %param.24) | copy-start | bytes 6148
  210.0 17.7 %copy-start.8 = (bf16[2048,128]{1,0:T(8,128)(2,1)S(1)}, bf16[2048,128]{1,0:T(8,128)(2,1)}, u32[]{:S(2)}) copy-start(bf16[2048,128]{1,0:T(8,128)(2,1)} %param.19) | copy-start | bytes 1572868
  214.9 31.0 %all-to-all-start.2 = ((bf16[16,2,1,32,128]{4,3,1,2,0:T(8,128)(2,1)}), bf16[16,2,1,32,128]{4,3,1,2,0:T(8,128)(2,1)S(1)}, u32[]{:S(2)}, u32[]{:S(2)}) async-start(bf16[16,2,1,32,128]{4,3,1,2,0:T(8,128)(2,1)} %copy.51), calls=%async_computation.2 | async-start | bytes 524288 | tf_op jit(solution)/shard_map/all_to_all | solution.py:47
Sparse Core Ops, SparseCore 0:
  57.5 71.5 all-gather.2
  134.9 71.5 all-gather.4
where the time goes:
time: 255 us
  waiting for transfers between devices  171 us (67%)
  starting transfers between devices  32.6 us (13%)
  between operations  14.5 us (6%)
  matrix products  13.4 us (5%)
  local copies, waits for them, and re-layouts  11 us (4%)
  other arithmetic  8.38 us (3%)
  blocking collectives  4.08 us (2%)
    all_gather x1, waiting for transfers between devices, shards(): lax.all_gather(hidden, 'tp', axis=1, tiled=True)  71.7 us
    all_gather x1, waiting for transfers between devices, side_by_side(): whole = lax.all_gather(both, axis, axis=dim, tiled=True)  71.7 us
    all_to_all x1, waiting for transfers between devices, exchange_in_order(): whole = lax.all_to_all(whole, axes[k], k, k, tiled=True)  15.9 us
    all_to_all x1, starting transfers between devices, shards(): lax.all_to_all(outgoing, EP, split_axis=0, concat_axis=0, tiled=True)  15.5 us
    all_to_all x1, starting transfers between devices, exchange_in_order(): whole = lax.all_to_all(whole, axes[k], k, k, tiled=True)  12.7 us
    dot_general x4, matrix products, add_product(): return jnp.dot(piece, weight, preferred_element_type=jnp.float32)  11.3 us
    all_to_all x1, waiting for transfers between devices, shards(): lax.all_to_all(outgoing, EP, split_axis=0, concat_axis=0, tiled=True)  8.72 us
  transfers between devices with their start and end apart: 6, of which 5 were waited for; matrix products, arithmetic and copies ran while one was open for 3% of the time, Pallas kernels for 0%

commit v1 on v0

--- a/solution.py
+++ b/solution.py
@@ -13,6 +13,12 @@
 LIMIT = 7.0
 SLOPE = 1.702
 BASE = 10000.0
+
+
+def gather_by_exchange(x, axis, dim):
+    count = lax.axis_size(axis)
+    repeats = [count if d == dim else 1 for d in range(x.ndim)]
+    return lax.all_to_all(jnp.tile(x, repeats), axis, split_axis=dim, concat_axis=dim, tiled=True)
 
 
 def extended(shard, sides, width):
@@ -197,7 +203,7 @@
     gate = add_product(feature_piece, gate_local)
     up = add_product(feature_piece, up_local)
     hidden = activate(gate, up)
-    result = add_product(lax.all_gather(hidden, "tp", axis=1, tiled=True), down_local)
+    result = add_product(gather_by_exchange(hidden, "tp", 1), down_local)
     result = result.astype(jnp.bfloat16).reshape(experts, capacity, down_local.shape[1])
     returned = exchange_by_chip(result, ("ep_0", "ep_1"), (1, 0), 0, 0)
     mixer_output = mixer_total.astype(jnp.bfloat16)

time: 255 us -> 246 us (0.965)
  the two profiles are of different devices: /device:TPU:32 before, /device:TPU:2 now
where the time goes in v1:
time: 246 us; the launch traced here: 245 us
  waiting for transfers between devices  99.4 us (40%)
  blocking collectives  59.8 us (24%)
  starting transfers between devices  32.1 us (13%)
  local copies, waits for them, and re-layouts  18.3 us (7%)
  between operations  14.5 us (6%)
  matrix products  12.9 us (5%)
  other arithmetic  8.36 us (3%)
    all_gather x1, waiting for transfers between devices, side_by_side(): whole = lax.all_gather(both, axis, axis=dim, tiled=True)  69.7 us
    all_to_all x1, blocking collectives, gather_by_exchange(): lax.all_to_all(jnp.tile(x, repeats), axis, split_axis=dim, concat_axis=di...  55.8 us
    all_to_all x1, waiting for transfers between devices, exchange_in_order(): whole = lax.all_to_all(whole, axes[k], k, k, tiled=True)  16 us
    all_to_all x1, starting transfers between devices, shards(): lax.all_to_all(outgoing, EP, split_axis=0, concat_axis=0, tiled=True)  15.5 us
    all_to_all x1, waiting for transfers between devices, shards(): lax.all_to_all(outgoing, EP, split_axis=0, concat_axis=0, tiled=True)  13.6 us
    all_to_all x1, starting transfers between devices, exchange_in_order(): whole = lax.all_to_all(whole, axes[k], k, k, tiled=True)  12.3 us
    dot_general x4, matrix products, add_product(): return jnp.dot(piece, weight, preferred_element_type=jnp.float32)  10.7 us
    all_to_all x1, local copies, waits for them, and re-layouts, gather_by_exchange(): lax.all_to_all(jnp.tile(x, repeats), axis, split_axis=dim, concat_axis=di...  6.51 us
  transfers between devices with their start and end apart: 5, of which 3 were waited for; matrix products, arithmetic and copies ran while one was open for 3% of the time, Pallas kernels for 0%

profile of v1, /device:TPU:2, one launch (start us, length us, event | category | flops | bytes accessed | tf_op | source)
XLA Modules:
  0.0 245.3 jit_solution(1807772073622336707)
XLA Ops:
  7.2 0.8 broadcast_multiply_fusion
  8.0 0.8 copy.63
  9.0 1.2 fusion.26
  10.5 1.2 reduce-window.6
  12.1 2.4 scatter_custom_fusion
  14.6 1.2 fusion.28
  15.8 4.3 %gather_fusion = bf16[1024,128]{1,0:T(8,128)(2,1)} fusion(bf16[129,128]{1,0:T(8,128)(2,1)S(1)} %pad_dynamic-slice_fusion, s32[1024]{0:T(1024)S(1)} %fusion.69), kind=kCustom, calls=%fused_computation | custom fusion | bytes 528384 | tf_op jit(solution)/shard_map/gather | solution.py:198
  20.1 15.5 %all-to-all-start = ((bf16[32,32,128]{2,1,0:T(8,128)(2,1)}), bf16[32,32,128]{2,1,0:T(8,128)(2,1)S(1)}, u32[]{:S(2)}, u32[]{:S(2)}) async-start(bf16[32,32,128]{2,1,0:T(8,128)(2,1)} %bitcast.20), calls=%async_computation | async-start | bytes 524288 | tf_op jit(solution)/shard_map/all_to_all | solution.py:199
  37.6 1.3 collective-permute-start.1
  38.9 3.0 %collective-permute-start = (bf16[128,128]{0,1:T(8,128)(2,1)S(1)}, bf16[128,128]{0,1:T(8,128)(2,1)S(1)}, u32[]{:S(2)}, u32[]{:S(2)}) collective-permute-start(bf16[128,128]{0,1:T(8,128)(2,1)S(1)} %get-tuple-element.11), channel_id=1, source_target_pairs={{0,16},{16,32},{32,48},{48,64},{64,80},{80,96},{96,112},{112,128},... | collective-permute-start | bytes 98312 | tf_op jit(solution)/shard_map/ppermute | solution.py:31
  44.9 13.6 %all-to-all-done = bf16[32,32,128]{2,1,0:T(8,128)(2,1)S(1)} async-done(((bf16[32,32,128]{2,1,0:T(8,128)(2,1)}), bf16[32,32,128]{2,1,0:T(8,128)(2,1)S(1)}, u32[]{:S(2)}, u32[]{:S(2)}) %all-to-all-start) | async-done | bytes 262176 | tf_op jit(solution)/shard_map/all_to_all | solution.py:199
  59.3 69.7 %all-gather.2.cloned.1.call-done = bf16[1280,2048]{1,0:T(8,128)(2,1)} async-done(((bf16[1280,128]{1,0:T(8,128)(2,1)}), bf16[1280,2048]{1,0:T(8,128)(2,1)}) %all-gather.2.cloned.1.call-update) | async-done | bytes 5242896 | tf_op jit(solution)/shard_map/all_gather | solution.py:66
  129.0 3.6 %fusion.8 = f32[1024,128]{1,0:T(8,128)S(1)} fusion(bf16[1280,2048]{1,0:T(8,128)(2,1)} %all-gather.2.cloned.1.call-done, bf16[1,2048,128]{2,1,0:T(8,128)(2,1)S(1)} %copy-done), kind=kOutput, calls=%fused_computation.16 | convolution fusion | flops 537001984 | bytes 5242880 | tf_op jit(solution)/shard_map/dot_general | solution.py:107
  132.7 1.3 fusion.21
  134.0 0.8 tile.2
  134.8 55.8 %all_to_all.24 = bf16[1024,16,128]{2,0,1:T(8,128)(2,1)} all-to-all(bf16[1024,16,128]{2,0,1:T(8,128)(2,1)S(1)} %tile.2), channel_id=1, replica_groups=mesh['ep_0'=16,'ep_1'=2,'tp'=16] {'tp'}, dimensions={1} | all-to-all | bytes 8388608 | tf_op jit(solution)/shard_map/all_to_all | solution.py:21
  190.6 6.5 %copy.67 = bf16[1024,16,128]{0,2,1:T(8,128)(2,1)} copy(bf16[1024,16,128]{2,0,1:T(8,128)(2,1)} %all_to_all.24) | data formatting | bytes 8388608 | tf_op jit(solution)/shard_map/all_to_all | solution.py:21
  197.1 3.6 %convolution_convert_fusion = bf16[1024,128]{1,0:T(8,128)(2,1)S(1)} fusion(bf16[1024,2048]{0,1:T(8,128)(2,1)} %bitcast.111, bf16[1,2048,128]{2,1,0:T(8,128)(2,1)S(1)} %copy-done.7), kind=kOutput, calls=%fused_computation.22 | convolution fusion | flops 537001984 | bytes 4980736 | tf_op jit(solution)/shard_map/dot_general | solution.py:107
  200.7 3.9 %all_to_all.25 = bf16[16,2,1,32,128]{4,3,0,2,1:T(8,128)(2,1)S(1)} all-to-all(bf16[16,2,1,32,128]{4,3,0,2,1:T(8,128)(2,1)S(1)} %copy.68), channel_id=1, replica_groups=mesh['ep_0'=16,'ep_1'=2,'tp'=16] {'ep_1'}, dimensions={1} | all-to-all | bytes 524288 | tf_op jit(solution)/shard_map/all_to_all | solution.py:53
  205.4 12.3 %all-to-all-start.3 = ((bf16[16,2,1,32,128]{4,3,1,2,0:T(8,128)(2,1)}), bf16[16,2,1,32,128]{4,3,1,2,0:T(8,128)(2,1)S(1)}, u32[]{:S(2)}, u32[]{:S(2)}) async-start(bf16[16,2,1,32,128]{4,3,1,2,0:T(8,128)(2,1)} %copy.69), calls=%async_computation.3 | async-start | bytes 524288 | tf_op jit(solution)/shard_map/all_to_all | solution.py:53
  217.9 2.3 convolution_convert_fusion.1
  220.2 16.0 %all-to-all-done.3 = bf16[16,2,1,32,128]{4,3,1,2,0:T(8,128)(2,1)S(1)} async-done(((bf16[16,2,1,32,128]{4,3,1,2,0:T(8,128)(2,1)}), bf16[16,2,1,32,128]{4,3,1,2,0:T(8,128)(2,1)S(1)}, u32[]{:S(2)}, u32[]{:S(2)}) %all-to-all-start.3) | async-done | bytes 262176 | tf_op jit(solution)/shard_map/all_to_all | solution.py:53
  236.2 1.3 gather_fusion.1
  237.5 0.9 fusion.37
  (87 shorter events, 7.4 us)
Async XLA Ops:
  7.2 121.8 %copy-start = (bf16[1,2048,128]{2,1,0:T(8,128)(2,1)S(1)}, bf16[1,2048,128]{2,1,0:T(8,128)(2,1)}, u32[]{:S(2)}) copy-start(bf16[1,2048,128]{2,1,0:T(8,128)(2,1)} %param.25) | copy-start | bytes 1572868
  7.2 28.5 %copy-start.1 = (bf16[256,2048]{1,0:T(8,128)(2,1)S(1)}, bf16[256,2048]{1,0:T(8,128)(2,1)}, u32[]{:S(2)}) copy-start(bf16[256,2048]{1,0:T(8,128)(2,1)} %param.14) | copy-start | bytes 3145732
  7.2 28.8 %copy-start.11 = (f32[2048]{0:T(1024)S(1)}, f32[2048]{0:T(1024)}, u32[]{:S(2)}) copy-start(f32[2048]{0:T(1024)} %param.15) | copy-start | bytes 24580
  7.2 28.8 %copy-start.9 = (bf16[2048,64]{0,1:T(8,128)(2,1)S(1)}, bf16[2048,64]{0,1:T(8,128)(2,1)}, u32[]{:S(2)}) copy-start(bf16[2048,64]{0,1:T(8,128)(2,1)} %param.17) | copy-start | bytes 786436
  10.3 26.8 %copy-start.10 = (bf16[2048,64]{0,1:T(8,128)(2,1)S(1)}, bf16[2048,64]{0,1:T(8,128)(2,1)}, u32[]{:S(2)}) copy-start(bf16[2048,64]{0,1:T(8,128)(2,1)} %param.18) | copy-start | bytes 786436
  15.8 26.5 %copy-start.5 = (bf16[2048,128]{1,0:T(8,128)(2,1)S(1)}, bf16[2048,128]{1,0:T(8,128)(2,1)}, u32[]{:S(2)}) copy-start(bf16[2048,128]{1,0:T(8,128)(2,1)} %param.16) | copy-start | bytes 1572868
  20.1 38.4 %all-to-all-start = ((bf16[32,32,128]{2,1,0:T(8,128)(2,1)}), bf16[32,32,128]{2,1,0:T(8,128)(2,1)S(1)}, u32[]{:S(2)}, u32[]{:S(2)}) async-start(bf16[32,32,128]{2,1,0:T(8,128)(2,1)} %bitcast.20), calls=%async_computation | async-start | bytes 524288 | tf_op jit(solution)/shard_map/all_to_all | solution.py:199
  35.6 93.4 %all-gather.2.cloned.1.call-start = ((), (), s32[]{:S(2)}) async-start(), calls=%async_computation.4 | async-start | bytes 5570560 | tf_op jit(solution)/shard_map/all_gather | solution.py:66
  36.5 7.5 %copy-start.3 = (f32[2]{0:T(128)S(1)}, f32[2]{0:T(128)}, u32[]{:S(2)}) copy-start(f32[2]{0:T(128)} %param.20) | copy-start | bytes 28
  37.6 5.9 %collective-permute-start.1 = (bf16[128,128]{0,1:T(8,128)(2,1)S(1)}, bf16[128,128]{0,1:T(8,128)(2,1)S(1)}, u32[]{:S(2)}, u32[]{:S(2)}) collective-permute-start(bf16[128,128]{0,1:T(8,128)(2,1)S(1)} %get-tuple-element.10), channel_id=1, source_target_pairs={{16,0},{32,16},{48,32},{64,48},{80,64},{96,80},{112,96},{128,112},... | collective-permute-start | bytes 98312 | tf_op jit(solution)/shard_map/ppermute | solution.py:32
  38.9 4.6 %collective-permute-start = (bf16[128,128]{0,1:T(8,128)(2,1)S(1)}, bf16[128,128]{0,1:T(8,128)(2,1)S(1)}, u32[]{:S(2)}, u32[]{:S(2)}) collective-permute-start(bf16[128,128]{0,1:T(8,128)(2,1)S(1)} %get-tuple-element.11), channel_id=1, source_target_pairs={{0,16},{16,32},{32,48},{48,64},{64,80},{80,96},{96,112},{112,128},... | collective-permute-start | bytes 98312 | tf_op jit(solution)/shard_map/ppermute | solution.py:31
  59.2 73.3 %copy-start.6 = (bf16[1,2048,128]{2,1,0:T(8,128)(2,1)S(1)}, bf16[1,2048,128]{2,1,0:T(8,128)(2,1)}, u32[]{:S(2)}) copy-start(bf16[1,2048,128]{2,1,0:T(8,128)(2,1)} %param.26) | copy-start | bytes 1572868
  129.0 3.7 %copy-start.4 = (bf16[1280,2048]{1,0:T(8,128)(2,1)S(1)}, bf16[1280,2048]{1,0:T(8,128)(2,1)}, u32[]{:S(2)}) copy-start(bf16[1280,2048]{1,0:T(8,128)(2,1)} %all-gather.2.cloned.1.call-done) | copy-start | bytes 15728644
  190.6 6.5 %copy-start.7 = (bf16[1,2048,128]{2,1,0:T(8,128)(2,1)S(1)}, bf16[1,2048,128]{2,1,0:T(8,128)(2,1)}, u32[]{:S(2)}) copy-start(bf16[1,2048,128]{2,1,0:T(8,128)(2,1)} %param.27) | copy-start | bytes 1572868
  197.1 20.6 %copy-start.2 = (f32[128,4]{0,1:T(4,128)S(1)}, f32[128,4]{0,1:T(4,128)}, u32[]{:S(2)}) copy-start(f32[128,4]{0,1:T(4,128)} %param.24) | copy-start | bytes 6148
  197.1 20.8 %copy-start.8 = (bf16[2048,128]{1,0:T(8,128)(2,1)S(1)}, bf16[2048,128]{1,0:T(8,128)(2,1)}, u32[]{:S(2)}) copy-start(bf16[2048,128]{1,0:T(8,128)(2,1)} %param.19) | copy-start | bytes 1572868
  205.4 30.8 %all-to-all-start.3 = ((bf16[16,2,1,32,128]{4,3,1,2,0:T(8,128)(2,1)}), bf16[16,2,1,32,128]{4,3,1,2,0:T(8,128)(2,1)S(1)}, u32[]{:S(2)}, u32[]{:S(2)}) async-start(bf16[16,2,1,32,128]{4,3,1,2,0:T(8,128)(2,1)} %copy.69), calls=%async_computation.3 | async-start | bytes 524288 | tf_op jit(solution)/shard_map/all_to_all | solution.py:53
Sparse Core Ops, SparseCore 0:
  59.4 69.5 all-gather.1
